TPU v7x, 32 devices: a whole 2x2x4 slice. The times are simulated.
32 devices in a mesh: rep: 2 (over x), fs: 8 (over z, y), tp: 2 (over core).
Axes of the slice: x: 2, y: 2, z: 4, core: 2. Of those that a mesh axis runs over, the one named last changes fastest.
Arguments:
- tokens: bfloat16 [16, 1024, 2048], P(('rep', 'fs'), 'tp'), may hold values from -6 to 6
- mix_gain: float32 [2048], replicated, may hold values from 0.1 to 1.9
- out_gate_w: float32 [2048, 1024], P('fs', 'tp'), may hold values from -0.125 to 0.125
- in_gate_w: float32 [2048, 1024], P('fs', 'tp'), may hold values from -0.125 to 0.125
- value_w: float32 [2048, 1024], P('fs', 'tp'), may hold values from -0.125 to 0.125
- out_gate_scale: float32 [1024], P(('tp', 'fs')), may hold values from 0.28 to 3.5
- in_gate_scale: float32 [1024], P(('tp', 'fs')), may hold values from 0.5 to 2
- value_scale: float32 [1024], P(('tp', 'fs')), may hold values from 0.5 to 2
- mix_taps: float32 [3, 1024], P(None, 'tp'), may hold values from -3.5 to 3.5
- conv_gain: float32 [1024], P('tp'), may hold values from 0.1 to 1.9
- out_proj_w: float32 [1024, 2048], P('tp', 'fs'), may hold values from -0.1875 to 0.1875
- proj_scale: float32 [2048], P('fs'), may hold values from 0.5 to 2
- ffn_gain: float32 [2048], replicated, may hold values from 0.1 to 1.9
- gate_w: float32 [2048, 2816], P('fs', 'tp'), may hold values from -0.125 to 0.125
- up_w: float32 [2048, 2816], P('fs', 'tp'), may hold values from -0.125 to 0.125
- gate_scale: float32 [2816], P(('tp', 'fs')), may hold values from 0.5 to 2
- up_scale: float32 [2816], P(('tp', 'fs')), may hold values from 0.5 to 2
- gate_taps: float32 [3, 2816], P(None, 'tp'), may hold values from -3.5 to 3.5
- up_taps: float32 [3, 2816], P(None, 'tp'), may hold values from -3.5 to 3.5
- gate_bias: float32 [2816], P('tp'), may hold values from -3 to 3
- up_bias: float32 [2816], P('tp'), may hold values from -3 to 3
- down_w: float32 [2816, 2048], P('tp', 'fs'), may hold values from -0.109375 to 0.109375
- down_scale: float32 [2048], P('fs'), may hold values from 0.5 to 2
Outputs:
- layer_out: bfloat16 [16, 1024, 2048], P(('rep', 'fs'), 'tp')
All inputs are finite; a program needn't handle non-finite values.
Results may differ from a plain program's by a relative error of at most 0.02.
Values may be sent and summed in bfloat16 or wider, within the bound.
A program may use at most 128 MiB of HBM per device.

v0:
```python
import jax
import jax.numpy as jnp
from jax import lax
from jax.sharding import PartitionSpec as P

epsilon = 1e-06


def norm_rows(values, gain):
    return values * lax.rsqrt(jnp.mean(values * values, axis=-1, keepdims=True) + epsilon) * gain


def causal_taps(values, taps):
    kernel = taps.shape[0]
    length = values.shape[0]
    padded = jnp.pad(values, ((kernel - 1, 0), (0, 0)))
    total = jnp.zeros(values.shape, jnp.float32)
    for offset in range(kernel):
        total = total + taps[offset] * padded[offset : offset + length]
    return total


def column_block(left, scale_all, piece):
    return jnp.dot(left, piece, preferred_element_type=jnp.float32) * scale_all


def local(
    tokens,
    mix_gain,
    out_gate_w,
    in_gate_w,
    value_w,
    out_gate_scale,
    in_gate_scale,
    value_scale,
    mix_taps,
    conv_gain,
    out_proj_w,
    proj_scale,
    ffn_gain,
    gate_w,
    up_w,
    gate_scale,
    up_scale,
    gate_taps,
    up_taps,
    gate_bias,
    up_bias,
    down_w,
    down_scale,
):
    resid = tokens[0].astype(jnp.float32)
    normed_in = norm_rows(resid, mix_gain).astype(jnp.bfloat16)
    all_rows = lax.all_gather(normed_in, "tp", axis=0, tiled=True)
    whole_outgate, whole_ingate, whole_value, whole_gate, whole_up, whole_proj, whole_down = (
        lax.all_gather(out_gate_scale, "fs", axis=0, tiled=True),
        lax.all_gather(in_gate_scale, "fs", axis=0, tiled=True),
        lax.all_gather(value_scale, "fs", axis=0, tiled=True),
        lax.all_gather(gate_scale, "fs", axis=0, tiled=True),
        lax.all_gather(up_scale, "fs", axis=0, tiled=True),
        lax.all_gather(proj_scale, "fs", axis=0, tiled=True),
        lax.all_gather(down_scale, "fs", axis=0, tiled=True),
    )
    outgate_rows, ingate_rows, value_rows = (
        lax.all_gather(out_gate_w.astype(jnp.bfloat16), "fs", axis=0, tiled=True),
        lax.all_gather(in_gate_w.astype(jnp.bfloat16), "fs", axis=0, tiled=True),
        lax.all_gather(value_w.astype(jnp.bfloat16), "fs", axis=0, tiled=True),
    )
    out_gate = (
        jnp.dot(all_rows, outgate_rows, preferred_element_type=jnp.float32) * whole_outgate
    ).astype(jnp.bfloat16)
    in_gate = (
        jnp.dot(all_rows, ingate_rows, preferred_element_type=jnp.float32) * whole_ingate
    ).astype(jnp.bfloat16)
    value_in = (
        jnp.dot(all_rows, value_rows, preferred_element_type=jnp.float32) * whole_value
    ).astype(jnp.bfloat16)
    mixed_in = in_gate.astype(jnp.float32) * value_in.astype(jnp.float32)
    conv_out = (out_gate.astype(jnp.float32) * causal_taps(mixed_in, mix_taps)).astype(jnp.bfloat16)
    conv_float = conv_out.astype(jnp.float32)
    channels = conv_float.shape[1] * lax.axis_size("tp")
    sumsq = lax.psum(jnp.sum(conv_float * conv_float, axis=1), "tp")
    mixed = (conv_float * lax.rsqrt(sumsq / channels + epsilon)[:, None] * conv_gain).astype(
        jnp.bfloat16
    )
    partial_mix = column_block(
        mixed, whole_proj, lax.all_gather(out_proj_w.astype(jnp.bfloat16), "fs", axis=1, tiled=True)
    )
    summed = lax.psum_scatter(
        partial_mix.astype(jnp.bfloat16), "tp", scatter_dimension=0, tiled=True
    ).astype(jnp.float32)
    first = (resid + summed).astype(jnp.bfloat16)
    resid_two = first.astype(jnp.float32)
    normed_ffn = norm_rows(resid_two, ffn_gain).astype(jnp.bfloat16)
    ffn_all = lax.all_gather(normed_ffn, "tp", axis=0, tiled=True)
    gate_cast = gate_w.astype(jnp.bfloat16)
    up_cast = up_w.astype(jnp.bfloat16)
    gate_full, up_full = (
        lax.all_gather(gate_cast, "fs", axis=0, tiled=True),
        lax.all_gather(up_cast, "fs", axis=0, tiled=True),
    )
    gate_sum = jnp.dot(ffn_all, gate_full, preferred_element_type=jnp.float32)
    up_sum = jnp.dot(ffn_all, up_full, preferred_element_type=jnp.float32)
    gate_pre = (gate_sum * whole_gate).astype(jnp.bfloat16)
    up_pre = (up_sum * whole_up).astype(jnp.bfloat16)
    gate_act = causal_taps(gate_pre.astype(jnp.float32), gate_taps) + gate_bias
    up_act = causal_taps(up_pre.astype(jnp.float32), up_taps) + up_bias
    hidden = (jax.nn.silu(gate_act) * up_act).astype(jnp.bfloat16)
    partial_down = column_block(
        hidden, whole_down, lax.all_gather(down_w.astype(jnp.bfloat16), "fs", axis=1, tiled=True)
    )
    summed_two = lax.psum_scatter(
        partial_down.astype(jnp.bfloat16), "tp", scatter_dimension=0, tiled=True
    ).astype(jnp.float32)
    return (resid_two + summed_two).astype(jnp.bfloat16)[None]


def solution(mesh):
    placed = (
        P(("rep", "fs"), "tp", None),
        P(),
        P("fs", "tp"),
        P("fs", "tp"),
        P("fs", "tp"),
        P(("tp", "fs")),
        P(("tp", "fs")),
        P(("tp", "fs")),
        P(None, "tp"),
        P("tp"),
        P("tp", "fs"),
        P("fs"),
        P(),
        P("fs", "tp"),
        P("fs", "tp"),
        P(("tp", "fs")),
        P(("tp", "fs")),
        P(None, "tp"),
        P(None, "tp"),
        P("tp"),
        P("tp"),
        P("tp", "fs"),
        P("fs"),
    )
    return jax.shard_map(
        local, mesh=mesh, in_specs=placed, out_specs=P(("rep", "fs"), "tp", None), check_vma=False
    )
```

profile of v0, /device:TPU:0, one launch (start us, length us, event | category | flops | bytes accessed | tf_op | source)
XLA Modules:
  0.0 588.5 jit_solution(1970027633098902979)
XLA Ops:
  6.5 1.9 convert_element_type.110
  8.5 0.0 all-gather.18.cloned.1.call-update
  8.5 0.0 all-gather.12.cloned.1.call-start
  8.6 2.1 fusion.4
  10.7 0.0 copy-start.18
  10.8 2.7 fusion.6
  13.5 0.0 all-gather.12.cloned.1.call-update
  13.5 0.0 all-gather.16.cloned.1.call-start
  13.6 0.7 convert_element_type.107
  14.3 0.0 all-gather.16.cloned.1.call-update
  14.4 0.0 all-gather.14.cloned.1.call-start
  14.4 0.7 convert_element_type.104
  15.2 0.0 all-gather.14.cloned.1.call-update
  15.2 0.0 all-gather.20.cloned.1.call-start
  15.2 1.8 convert_element_type.116
  17.0 0.0 all-gather.20.cloned.1.call-update
  17.0 0.0 reduce-scatter.3.cloned.1.call-start
  17.1 0.6 dynamic-slice
  19.0 0.2 dynamic-update-slice
  19.2 0.2 dynamic-update-slice.1
  19.5 0.2 dynamic-update-slice.2
  19.7 0.3 dynamic-update-slice.3
  20.0 0.3 dynamic-update-slice.4
  20.2 40.2 %all-reduce.8 = (f32[512]{0:T(512)S(1)}, f32[512]{0:T(512)S(1)}, f32[512]{0:T(512)S(1)}, f32[1408]{0:T(1024)S(1)}, f32[1408]{0:T(1024)}) all-reduce(f32[512]{0:T(512)S(1)} %dynamic-update-slice.2, f32[512]{0:T(512)S(1)} %dynamic-update-slice.1, f32[512]{0:T(512)S(1)} %dynamic-update-slice, ...), channel_id=1, replica_groups=mesh['rep'=2,'fs'=8,'tp'=2] {'fs'}, use_global_device_ids=true, to_apply=%add.5 | all-reduce | flops 4352 | bytes 34816
  60.5 16.3 %all-gather = f32[8,1,256]{2,1,0:T(1,128)S(1)} all-gather(f32[1,1,256]{2,1,0:T(1,128)S(1)} %bitcast.39), channel_id=1, replica_groups=mesh['rep'=2,'fs'=8,'tp'=2] {'fs'}, dimensions={0}, use_global_device_ids=true | all-gather | bytes 9216 | tf_op jit(solution)/shard_map/all_gather | solution.py:61
  76.8 0.0 all-gather.18.cloned.1.call-done
  76.8 0.0 all-gather.12.cloned.1.call-done
  76.8 6.3 %multiply_convert_fusion.6 = bf16[1024,512]{0,1:T(8,128)(2,1)} fusion(bf16[1024,2048]{1,0:T(8,128)(2,1)} %all-gather.12.cloned.1.call-done, bf16[2048,512]{1,0:T(8,128)(2,1)} %all-gather.18.cloned.1.call-done, f32[512]{0:T(512)S(1)} %get-tuple-element.11), kind=kOutput, calls=%fused_computation.36 | convolution fusion | flops 2148532224 | bytes 7342080 | tf_op jit(solution)/shard_map/dot_general | solution.py:76
  83.1 44.9 %all-gather.16.cloned.1.call-done = bf16[2048,512]{1,0:T(8,128)(2,1)} async-done(((bf16[256,512]{1,0:T(8,128)(2,1)}), bf16[2048,512]{1,0:T(8,128)(2,1)}) %all-gather.16.cloned.1.call-update) | async-done | bytes 2097168 | tf_op jit(solution)/shard_map/all_gather | solution.py:66
  128.1 6.8 %convert_multiply_fusion.6 = f32[1024,512]{0,1:T(8,128)} fusion(bf16[1024,512]{0,1:T(8,128)(2,1)} %multiply_convert_fusion.6, bf16[1024,2048]{1,0:T(8,128)(2,1)} %all-gather.12.cloned.1.call-done, bf16[2048,512]{1,0:T(8,128)(2,1)} %all-gather.16.cloned.1.call-done, f32[512]{0:T(512)S(1)} %get-tuple-element.12), kind=kOutput, calls=%fused_computation.35 | convolution fusion | flops 2150105088 | bytes 9439232 | tf_op jit(solution)/shard_map/dot_general | solution.py:73
  134.8 42.9 %all-gather.14.cloned.1.call-done = bf16[2048,512]{1,0:T(8,128)(2,1)} async-done(((bf16[256,512]{1,0:T(8,128)(2,1)}), bf16[2048,512]{1,0:T(8,128)(2,1)}) %all-gather.14.cloned.1.call-update) | async-done | bytes 2097168 | tf_op jit(solution)/shard_map/all_gather | solution.py:65
  177.7 8.5 %fusion.16 = (f32[1024]{0:T(1024)S(1)}, bf16[1024,512]{0,1:T(8,128)(2,1)}) fusion(f32[1024,512]{0,1:T(8,128)} %convert_multiply_fusion.6, f32[512]{0:T(512)S(1)} %bitcast.37, f32[512]{0:T(512)S(1)} %bitcast.38, f32[512]{0:T(512)S(1)} %bitcast.36, f32[512]{0:T(512)S(1)} %get-tuple-element.13, bf16[1024,2048]{1,0:T(8,128)(2,1)} %all-gather.12.cloned.1.call-done, ...), kind=kOutput, calls=%fused_computation.31 | convolution fusion | flops 2154298368 | bytes 9449472 | tf_op jit(solution)/shard_map/dot_general | solution.py:70
  186.2 2.4 psum.7
  188.6 39.9 %all-gather.20.cloned.1.call-done = bf16[512,2048]{1,0:T(8,128)(2,1)} async-done(((bf16[512,256]{1,0:T(8,128)(2,1)}), bf16[512,2048]{1,0:T(8,128)(2,1)}) %all-gather.20.cloned.1.call-update) | async-done | bytes 2097168 | tf_op jit(solution)/shard_map/all_gather | solution.py:87
  228.5 6.4 %multiply_convert_fusion.1 = bf16[1024,2048]{1,0:T(8,128)(2,1)} fusion(bf16[512,2048]{1,0:T(8,128)(2,1)} %all-gather.20.cloned.1.call-done, f32[2048]{0:T(1024)S(1)} %bitcast.34, bf16[1024,512]{0,1:T(8,128)(2,1)} %get-tuple-element.20, f32[512]{0:T(512)S(1)} %copy-done.14, f32[1024]{0:T(1024)S(1)} %add_rsqrt_fusion), kind=kOutput, calls=%fused_computation.1 | convolution fusion | flops 2153775104 | bytes 7354368 | tf_op jit(solution)/shard_map/dot_general | solution.py:24
  234.9 0.0 reduce-scatter.3.cloned.1.call-update
  234.9 0.0 all-gather.24.cloned.1.call-start
  234.9 1.3 copy-done.2
  236.2 1.0 convert_element_type.122
  237.2 0.0 all-gather.24.cloned.1.call-update
  237.2 0.0 all-gather.22.cloned.1.call-start
  237.2 8.0 %reduce-scatter.3.cloned.1.call-done = bf16[512,2048]{1,0:T(8,128)(2,1)} async-done(((bf16[1024,2048]{1,0:T(8,128)(2,1)}), bf16[512,2048]{1,0:T(8,128)(2,1)}) %reduce-scatter.3.cloned.1.call-update) | async-done | bytes 2097168 | tf_op jit(solution)/shard_map/reduce_scatter | solution.py:89
  245.3 2.5 fusion
  247.8 2.4 fusion.2
  250.2 0.0 all-gather.22.cloned.1.call-update
  250.2 0.0 all-gather.26.cloned.1.call-start
  250.3 0.9 convert_element_type.125
  251.2 0.0 all-gather.26.cloned.1.call-update
  251.2 0.0 all-gather.28.cloned.1.call-start
  251.3 2.4 convert_element_type.129
  253.6 0.0 all-gather.28.cloned.1.call-update
  253.7 0.0 reduce-scatter.5.cloned.1.call-start
  253.7 21.6 %all-gather.1 = f32[8,1,256]{2,1,0:T(1,128)S(1)} all-gather(f32[1,1,256]{2,1,0:T(1,128)S(1)} %bitcast.40), channel_id=1, replica_groups=mesh['rep'=2,'fs'=8,'tp'=2] {'fs'}, dimensions={0}, use_global_device_ids=true | all-gather | bytes 9216 | tf_op jit(solution)/shard_map/all_gather | solution.py:62
  275.3 1.0 slice_reduce_fusion.2
  276.3 64.9 %all-gather.24.cloned.1.call-done = bf16[2048,1408]{1,0:T(8,128)(2,1)} async-done(((bf16[256,1408]{1,0:T(8,128)(2,1)}), bf16[2048,1408]{1,0:T(8,128)(2,1)}) %all-gather.24.cloned.1.call-update) | async-done | bytes 5767184 | tf_op jit(solution)/shard_map/all_gather | solution.py:99
  341.1 13.4 %all-gather.22.cloned.1.call-done = bf16[1024,2048]{1,0:T(8,128)(2,1)} async-done(((bf16[512,2048]{1,0:T(8,128)(2,1)}), bf16[1024,2048]{1,0:T(8,128)(2,1)}) %all-gather.22.cloned.1.call-update) | async-done | bytes 4194320 | tf_op jit(solution)/shard_map/all_gather | solution.py:95
  354.6 11.8 %fusion.8 = f32[1024,1408]{1,0:T(8,128)} fusion(bf16[1024,2048]{1,0:T(8,128)(2,1)} %all-gather.22.cloned.1.call-done, bf16[2048,1408]{1,0:T(8,128)(2,1)} %all-gather.24.cloned.1.call-done, f32[1408]{0:T(1024)} %get-tuple-element.15), kind=kOutput, calls=%fused_computation.19 | convolution fusion | flops 5909905408 | bytes 15734272 | tf_op jit(solution)/shard_map/dot_general | solution.py:102
  366.4 83.9 %all-gather.26.cloned.1.call-done = bf16[2048,1408]{1,0:T(8,128)(2,1)} async-done(((bf16[256,1408]{1,0:T(8,128)(2,1)}), bf16[2048,1408]{1,0:T(8,128)(2,1)}) %all-gather.26.cloned.1.call-update) | async-done | bytes 5767184 | tf_op jit(solution)/shard_map/all_gather | solution.py:100
  450.3 11.7 %fusion.9 = f32[1024,1408]{1,0:T(8,128)} fusion(bf16[1024,2048]{1,0:T(8,128)(2,1)} %all-gather.22.cloned.1.call-done, bf16[2048,1408]{1,0:T(8,128)(2,1)} %all-gather.26.cloned.1.call-done, f32[1408]{0:T(1024)S(1)} %get-tuple-element.14), kind=kOutput, calls=%fused_computation.20 | convolution fusion | flops 5909905408 | bytes 15734272 | tf_op jit(solution)/shard_map/dot_general | solution.py:103
  462.0 81.5 %all-gather.28.cloned.1.call-done = bf16[1408,2048]{1,0:T(8,128)(2,1)} async-done(((bf16[1408,256]{1,0:T(8,128)(2,1)}), bf16[1408,2048]{1,0:T(8,128)(2,1)}) %all-gather.28.cloned.1.call-update) | async-done | bytes 5767184 | tf_op jit(solution)/shard_map/all_gather | solution.py:110
  543.5 23.1 %multiply_convert_fusion = bf16[1024,2048]{1,0:T(8,128)(2,1)} fusion(bf16[1408,2048]{1,0:T(8,128)(2,1)} %all-gather.28.cloned.1.call-done, f32[2048]{0:T(1024)S(1)} %bitcast.35, f32[1024,1408]{1,0:T(8,128)} %fusion.9, f32[1024,1408]{1,0:T(8,128)} %fusion.8, f32[1408]{0:T(1024)S(1)} %copy-done.12, f32[1408]{0:T(1024)S(1)} %get-tuple-element.9, ...), kind=kOutput, calls=%fused_computation | convolution fusion | flops 5935726592 | bytes 21549056 | tf_op jit(solution)/shard_map/dot_general | solution.py:24
  566.6 0.0 reduce-scatter.5.cloned.1.call-update
  566.6 10.4 %reduce-scatter.5.cloned.1.call-done = bf16[512,2048]{1,0:T(8,128)(2,1)} async-done(((bf16[1024,2048]{1,0:T(8,128)(2,1)}), bf16[512,2048]{1,0:T(8,128)(2,1)}) %reduce-scatter.5.cloned.1.call-update) | async-done | bytes 2097168 | tf_op jit(solution)/shard_map/reduce_scatter | solution.py:112
  577.0 5.0 fusion.19
  (46 shorter events, 0.1 us)
Async XLA Ops:
  6.5 4.2 copy-start
  6.5 70.3 %all-gather.18.cloned.1.call-start = ((), (), s32[]{:S(2)}) async-start(), calls=%async_computation.5 | async-start | bytes 2359296 | tf_op jit(solution)/shard_map/all_gather | solution.py:67
  8.5 5.1 copy-start.4
  8.5 68.3 %all-gather.12.cloned.1.call-start = ((), (), s32[]{:S(2)}) async-start(), calls=%async_computation.2 | async-start | bytes 6291456 | tf_op jit(solution)/shard_map/all_gather | solution.py:54
  10.7 3.7 copy-start.5
  10.7 6.4 %copy-start.18 = (u32[32]{0:T(128)S(1)}, u32[32]{0:T(128)}, u32[]{:S(2)}) copy-start(u32[32]{0:T(128)} %constant.26) | copy-start | bytes 388
  10.7 8.2 %copy-start.15 = (f32[64]{0:T(128)S(1)}, f32[64]{0:T(128)}, u32[]{:S(2)}) copy-start(f32[64]{0:T(128)} %param.28) | copy-start | bytes 772
  10.7 8.5 %copy-start.16 = (f32[64]{0:T(128)S(1)}, f32[64]{0:T(128)}, u32[]{:S(2)}) copy-start(f32[64]{0:T(128)} %param.29) | copy-start | bytes 772
  10.8 8.7 %copy-start.17 = (f32[64]{0:T(128)S(1)}, f32[64]{0:T(128)}, u32[]{:S(2)}) copy-start(f32[64]{0:T(128)} %param.30) | copy-start | bytes 772
  10.8 8.9 %copy-start.10 = (f32[176]{0:T(256)S(1)}, f32[176]{0:T(256)}, u32[]{:S(2)}) copy-start(f32[176]{0:T(256)} %param.38) | copy-start | bytes 2116
  10.8 9.2 %copy-start.11 = (f32[176]{0:T(256)S(1)}, f32[176]{0:T(256)}, u32[]{:S(2)}) copy-start(f32[176]{0:T(256)} %param.39) | copy-start | bytes 2116
  10.8 49.7 %copy-start.8 = (f32[256]{0:T(256)S(1)}, f32[256]{0:T(256)}, u32[]{:S(2)}) copy-start(f32[256]{0:T(256)} %param.34) | copy-start | bytes 3076
  10.8 66.0 %copy-start.7 = (f32[3,512]{1,0:T(4,128)S(1)}, f32[3,512]{1,0:T(4,128)}, u32[]{:S(2)}) copy-start(f32[3,512]{1,0:T(4,128)} %param.31) | copy-start | bytes 18436
  13.5 114.5 %all-gather.16.cloned.1.call-start = ((), (), s32[]{:S(2)}) async-start(), calls=%async_computation.4 | async-start | bytes 2359296 | tf_op jit(solution)/shard_map/all_gather | solution.py:66
  14.4 163.3 %all-gather.14.cloned.1.call-start = ((), (), s32[]{:S(2)}) async-start(), calls=%async_computation.3 | async-start | bytes 2359296 | tf_op jit(solution)/shard_map/all_gather | solution.py:65
  15.2 213.3 %all-gather.20.cloned.1.call-start = ((), (), s32[]{:S(2)}) async-start(), calls=%async_computation.6 | async-start | bytes 2359296 | tf_op jit(solution)/shard_map/all_gather | solution.py:87
  17.0 228.2 %reduce-scatter.3.cloned.1.call-start = ((), (), s32[]{:S(2)}) async-start(), calls=%async_computation.7 | async-start | bytes 6291456 | tf_op jit(solution)/shard_map/reduce_scatter | solution.py:89
  177.7 50.8 %copy-start.14 = (f32[512]{0:T(512)S(1)}, f32[512]{0:T(512)}, u32[]{:S(2)}) copy-start(f32[512]{0:T(512)} %param.32) | copy-start | bytes 6148
  234.9 1.4 copy-start.2
  234.9 12.9 %copy-start.6 = (f32[2048]{0:T(1024)S(1)}, f32[2048]{0:T(1024)}, u32[]{:S(2)}) copy-start(f32[2048]{0:T(1024)} %param.35) | copy-start | bytes 24580
  234.9 106.3 %all-gather.24.cloned.1.call-start = ((), (), s32[]{:S(2)}) async-start(), calls=%async_computation.9 | async-start | bytes 6488064 | tf_op jit(solution)/shard_map/all_gather | solution.py:99
  237.2 117.4 %all-gather.22.cloned.1.call-start = ((), (), s32[]{:S(2)}) async-start(), calls=%async_computation.8 | async-start | bytes 6291456 | tf_op jit(solution)/shard_map/all_gather | solution.py:95
  245.3 2.5 copy-start.1
  247.8 2.5 copy-start.3
  250.2 3.5 copy-start.9
  250.2 200.1 %all-gather.26.cloned.1.call-start = ((), (), s32[]{:S(2)}) async-start(), calls=%async_computation.10 | async-start | bytes 6488064 | tf_op jit(solution)/shard_map/all_gather | solution.py:100
  251.2 292.3 %all-gather.28.cloned.1.call-start = ((), (), s32[]{:S(2)}) async-start(), calls=%async_computation.11 | async-start | bytes 6488064 | tf_op jit(solution)/shard_map/all_gather | solution.py:110
  253.7 323.3 %reduce-scatter.5.cloned.1.call-start = ((), (), s32[]{:S(2)}) async-start(), calls=%async_computation.12 | async-start | bytes 6291456 | tf_op jit(solution)/shard_map/reduce_scatter | solution.py:112
  450.3 93.2 %copy-start.12 = (f32[1408]{0:T(1024)S(1)}, f32[1408]{0:T(1024)}, u32[]{:S(2)}) copy-start(f32[1408]{0:T(1024)} %param.43) | copy-start | bytes 16900
  450.3 93.2 %copy-start.13 = (f32[1408]{0:T(1024)S(1)}, f32[1408]{0:T(1024)}, u32[]{:S(2)}) copy-start(f32[1408]{0:T(1024)} %param.42) | copy-start | bytes 16900
Sparse Core Ops, SparseCore 0:
  9.5 52.1 all-gather.17
  63.2 12.3 all-gather.11
  77.8 50.2 all-gather.15
  130.0 47.6 all-gather.13
  179.6 48.8 all-gather.19
  235.0 10.2 reduce-scatter.2
  247.4 93.6 all-gather.23
  342.7 11.8 all-gather.21
  356.8 93.4 all-gather.25
  452.2 91.3 all-gather.27
  566.7 10.2 reduce-scatter.4
where the time goes:
time: 589 us; the launch traced here: 588 us
  waiting for transfers between devices  390 us (66%)
  blocking collectives  80.6 us (14%)
  matrix products  74.4 us (13%)
  other arithmetic  24.1 us (4%)
  between operations  14.7 us (2%)
    all_gather x1, waiting for transfers between devices, local(): lax.all_gather(up_cast, 'fs', axis=0, tiled=True)  83.9 us
    all_gather x1, waiting for transfers between devices, local(): lax.all_gather(down_w.astype(jnp.bfloat16), 'fs', axis=1, tiled=True)  81.5 us
    all_gather x1, waiting for transfers between devices, local(): lax.all_gather(gate_cast, 'fs', axis=0, tiled=True)  64.9 us
    all_gather x1, waiting for transfers between devices, local(): lax.all_gather(in_gate_w.astype(jnp.bfloat16), 'fs', axis=0, tiled=True)  44.9 us
    all_gather x1, waiting for transfers between devices, local(): lax.all_gather(out_gate_w.astype(jnp.bfloat16), 'fs', axis=0, tiled=True)  42.9 us
    unnamed x1, blocking collectives  40.2 us
    all_gather x1, waiting for transfers between devices, local(): lax.all_gather(out_proj_w.astype(jnp.bfloat16), 'fs', axis=1, tiled=True)  39.9 us
    dot_general x2, matrix products, column_block(): return jnp.dot(left, piece, preferred_element_type=jnp.float32) * scale_all  29.4 us
  transfers between devices with their start and end apart: 11, of which 9 were waited for; matrix products, arithmetic and copies ran while one was open for 11% of the time, Pallas kernels for 0%

commit v1 on v0

--- a/solution.py
+++ b/solution.py
@@ -1,9 +1,210 @@
+import functools
+
 import jax
 import jax.numpy as jnp
 from jax import lax
+from jax.experimental import pallas as pl
+from jax.experimental.pallas import tpu as pltpu
 from jax.sharding import PartitionSpec as P
 
+MESH = pl.DeviceIdType.MESH
 epsilon = 1e-06
+
+
+def split_rows(rows, step):
+    a = max((rows * 3 // 8) // step, 1) * step
+    return a, rows - 2 * a
+
+
+class Gather:
+    def __init__(self, sizes, srcs, dsts, steps, sems):
+        self.srcs, self.dsts, self.steps = srcs, dsts, steps
+        self.fs = sizes["fs"]
+        self.ny = 2
+        self.nz = self.fs // self.ny
+        self.me = lax.axis_index("fs")
+        self.x = lax.axis_index("rep")
+        self.y = self.me % self.ny
+        self.z = self.me // self.ny
+        self.sz, self.rz, self.sy, self.ry, self.sx, self.rx = sems
+        self.left = {"fs": self.me - self.ny}
+        self.right = {"fs": self.me + self.ny}
+        self.across = {"fs": self.z * self.ny + 1 - self.y}
+        self.other = {"rep": 1 - self.x}
+
+    def barrier(self):
+        sem = pltpu.get_barrier_semaphore()
+        has_left = self.z > 0
+        has_right = self.z < self.nz - 1
+
+        @pl.when(has_left)
+        def _():
+            pl.semaphore_signal(sem, inc=1, device_id=self.left, device_id_type=MESH)
+
+        @pl.when(has_right)
+        def _():
+            pl.semaphore_signal(sem, inc=1, device_id=self.right, device_id_type=MESH)
+
+        pl.semaphore_signal(sem, inc=1, device_id=self.across, device_id_type=MESH)
+        pl.semaphore_signal(sem, inc=1, device_id=self.other, device_id_type=MESH)
+        pl.semaphore_wait(sem, 2 + has_left.astype(jnp.int32) + has_right.astype(jnp.int32))
+
+    def part(self, c, x, short):
+        rows = self.srcs[c].shape[0]
+        a, b = split_rows(rows, self.steps[c])
+        if short:
+            return pl.ds(pl.multiple_of(x * (a + b), self.steps[c]), a)
+        return pl.ds(pl.multiple_of(x * a, self.steps[c]), a + b)
+
+    def copy(self, c, origin, rows, send, recv, target, own=False):
+        dst = self.dsts[c].at[origin, rows]
+        return pltpu.make_async_remote_copy(
+            src_ref=self.srcs[c].at[rows] if own else dst,
+            dst_ref=dst,
+            send_sem=send,
+            recv_sem=recv,
+            device_id=target,
+            device_id_type=MESH,
+        )
+
+    def along(self, c, way, hop, own=False):
+        origin = self.me - (hop - 1) * self.ny if way == 0 else self.me + (hop - 1) * self.ny
+        target = self.right if way == 0 else self.left
+        return self.copy(
+            c, origin, self.part(c, self.x, False), self.sz.at[c, way, hop], self.rz.at[c, way, hop], target, own
+        )
+
+    def sends(self, way, hop):
+        if way == 0:
+            return (self.z < self.nz - 1) & (self.z - (hop - 1) >= 0)
+        return (self.z > 0) & (self.z + (hop - 1) <= self.nz - 1)
+
+    def arrives(self, way, hop):
+        return self.z - hop >= 0 if way == 0 else self.z + hop <= self.nz - 1
+
+    def over_y(self, c, slot, origin, own=False):
+        return self.copy(
+            c, origin, self.part(c, self.x, False), self.sy.at[c, slot], self.ry.at[c, slot], self.across, own
+        )
+
+    def over_x(self, c, slot, origin):
+        return self.copy(c, origin, self.part(c, self.x, True), self.sx.at[c, slot], self.rx.at[c, slot], self.other)
+
+    def origin(self, way, hop):
+        return self.me - hop * self.ny if way == 0 else self.me + hop * self.ny
+
+    def mirror(self, origin):
+        return origin + 1 - 2 * self.y
+
+    def start_own(self, c):
+        for way in range(2):
+            pl.when(self.sends(way, 1))(lambda way=way: self.along(c, way, 1, True).start())
+        self.over_y(c, 0, self.me, True).start()
+
+    def z_arrival(self, c, hop):
+        for way in range(2):
+            slot = 2 * hop - 1 + way
+            origin = self.origin(way, hop)
+
+            @pl.when(self.arrives(way, hop))
+            def _():
+                self.along(c, way, hop).wait_recv()
+                if hop < self.nz - 1:
+                    pl.when(self.sends(way, hop + 1))(lambda: self.along(c, way, hop + 1).start())
+                self.over_y(c, slot, origin).start()
+                self.over_x(c, slot, origin).start()
+
+    def y_arrival(self, c, hop):
+        for way in range(2 if hop else 1):
+            slot = 2 * hop - 1 + way if hop else 0
+            origin = self.mirror(self.origin(way, hop))
+
+            def go():
+                self.over_y(c, slot, origin).wait_recv()
+                self.over_x(c, 2 * self.nz + slot, origin).start()
+
+            pl.when(self.arrives(way, hop))(go) if hop else go()
+
+    def x_arrivals(self, c):
+        for hop in range(self.nz):
+            for way in range(2 if hop else 1):
+                slot = 2 * hop - 1 + way if hop else 0
+                near = self.origin(way, hop)
+
+                def go():
+                    for base, origin in ((0, near), (2 * self.nz, self.mirror(near))):
+                        if base or hop:
+                            rows = self.part(c, 1 - self.x, True)
+                            self.copy(
+                                c, origin, rows, self.sx.at[c, base + slot], self.rx.at[c, base + slot], self.other
+                            ).wait_recv()
+
+                pl.when(self.arrives(way, hop))(go) if hop else go()
+
+    def finish(self, c):
+        for hop in range(self.nz):
+            for way in range(2):
+                if hop + 1 < self.nz:
+                    pl.when(self.sends(way, hop + 1))(
+                        lambda way=way, hop=hop: self.along(c, way, hop + 1).wait_send()
+                    )
+                if hop == 0 and way == 1:
+                    continue
+                slot = 2 * hop - 1 + way if hop else 0
+                near = self.origin(way, hop)
+
+                def go():
+                    self.over_y(c, slot, near).wait_send()
+                    self.over_x(c, 2 * self.nz + slot, self.mirror(near)).wait_send()
+                    if hop:
+                        self.over_x(c, slot, near).wait_send()
+
+                pl.when(self.arrives(way, hop))(go) if hop else go()
+
+
+def gather_kernel(sizes, steps, count, *refs):
+    srcs, dsts = refs[:count], refs[count : 2 * count]
+    sems, own_sem = refs[2 * count : -1], refs[-1]
+    g = Gather(sizes, srcs, dsts, steps, sems)
+    own = [pltpu.make_async_copy(srcs[c], dsts[c].at[g.me], own_sem.at[c]) for c in range(count)]
+    g.barrier()
+    g.start_own(0)
+    for copy in own:
+        copy.start()
+    for c in range(count + 1):
+        if c + 1 < count:
+            g.start_own(c + 1)
+        for hop in range(g.nz):
+            if hop and c < count:
+                g.z_arrival(c, hop)
+            if c:
+                g.y_arrival(c - 1, hop)
+    for c in range(count):
+        g.x_arrivals(c)
+        g.finish(c)
+        own[c].wait()
+
+
+def gather_all(sizes, srcs, steps):
+    fs = sizes["fs"]
+    nz, count = fs // 2, len(srcs)
+    dma = pltpu.SemaphoreType.DMA
+    return pl.pallas_call(
+        functools.partial(gather_kernel, sizes, steps, count),
+        out_shape=[jax.ShapeDtypeStruct((fs,) + s.shape, s.dtype) for s in srcs],
+        in_specs=[pl.BlockSpec(memory_space=pl.ANY)] * count,
+        out_specs=[pl.BlockSpec(memory_space=pl.ANY)] * count,
+        scratch_shapes=[
+            dma((count, 2, nz)),
+            dma((count, 2, nz)),
+            dma((count, 2 * nz)),
+            dma((count, 2 * nz)),
+            dma((count, 4 * nz)),
+            dma((count, 4 * nz)),
+            dma((count,)),
+        ],
+        compiler_params=pltpu.CompilerParams(collective_id=0, has_side_effects=True),
+    )(*srcs)
 
 
 def norm_rows(values, gain):
@@ -25,6 +226,7 @@
 
 
 def local(
+    sizes,
     tokens,
     mix_gain,
     out_gate_w,
@@ -52,20 +254,33 @@
     resid = tokens[0].astype(jnp.float32)
     normed_in = norm_rows(resid, mix_gain).astype(jnp.bfloat16)
     all_rows = lax.all_gather(normed_in, "tp", axis=0, tiled=True)
-    whole_outgate, whole_ingate, whole_value, whole_gate, whole_up, whole_proj, whole_down = (
-        lax.all_gather(out_gate_scale, "fs", axis=0, tiled=True),
-        lax.all_gather(in_gate_scale, "fs", axis=0, tiled=True),
-        lax.all_gather(value_scale, "fs", axis=0, tiled=True),
-        lax.all_gather(gate_scale, "fs", axis=0, tiled=True),
-        lax.all_gather(up_scale, "fs", axis=0, tiled=True),
-        lax.all_gather(proj_scale, "fs", axis=0, tiled=True),
-        lax.all_gather(down_scale, "fs", axis=0, tiled=True),
-    )
+    vectors = [out_gate_scale, in_gate_scale, value_scale, gate_scale, up_scale, proj_scale, down_scale]
+    flat = jnp.concatenate(vectors)
+    lines = 24 * (-(-flat.shape[0] // (24 * 128)))
+    flat = jnp.pad(flat, (0, lines * 128 - flat.shape[0])).reshape(lines, 128)
+    half = jnp.bfloat16
+    mix_w = jnp.concatenate([out_gate_w.astype(half), in_gate_w.astype(half), value_w.astype(half)], axis=1)
+    flats, mix_all, proj_all, gate_all, up_all, down_all = gather_all(
+        sizes,
+        [flat, mix_w, out_proj_w.astype(half), gate_w.astype(half), up_w.astype(half), down_w.astype(half)],
+        [8, 16, 16, 16, 16, 16],
+    )
+    fs = sizes["fs"]
+    flats = flats.reshape(fs, -1)
+    scales, at = [], 0
+    for vector in vectors:
+        scales.append(flats[:, at : at + vector.shape[0]].reshape(-1))
+        at += vector.shape[0]
+    whole_outgate, whole_ingate, whole_value, whole_gate, whole_up, whole_proj, whole_down = scales
+    mix_full = mix_all.reshape(-1, mix_w.shape[1])
+    width = out_gate_w.shape[1]
     outgate_rows, ingate_rows, value_rows = (
-        lax.all_gather(out_gate_w.astype(jnp.bfloat16), "fs", axis=0, tiled=True),
-        lax.all_gather(in_gate_w.astype(jnp.bfloat16), "fs", axis=0, tiled=True),
-        lax.all_gather(value_w.astype(jnp.bfloat16), "fs", axis=0, tiled=True),
-    )
+        mix_full[:, :width],
+        mix_full[:, width : 2 * width],
+        mix_full[:, 2 * width :],
+    )
+    proj_cols = proj_all.transpose(1, 0, 2).reshape(proj_all.shape[1], -1)
+    down_cols = down_all.transpose(1, 0, 2).reshape(down_all.shape[1], -1)
     out_gate = (
         jnp.dot(all_rows, outgate_rows, preferred_element_type=jnp.float32) * whole_outgate
     ).astype(jnp.bfloat16)
@@ -84,7 +299,7 @@
         jnp.bfloat16
     )
     partial_mix = column_block(
-        mixed, whole_proj, lax.all_gather(out_proj_w.astype(jnp.bfloat16), "fs", axis=1, tiled=True)
+        mixed, whole_proj, proj_cols
     )
     summed = lax.psum_scatter(
         partial_mix.astype(jnp.bfloat16), "tp", scatter_dimension=0, tiled=True
@@ -93,12 +308,8 @@
     resid_two = first.astype(jnp.float32)
     normed_ffn = norm_rows(resid_two, ffn_gain).astype(jnp.bfloat16)
     ffn_all = lax.all_gather(normed_ffn, "tp", axis=0, tiled=True)
-    gate_cast = gate_w.astype(jnp.bfloat16)
-    up_cast = up_w.astype(jnp.bfloat16)
-    gate_full, up_full = (
-        lax.all_gather(gate_cast, "fs", axis=0, tiled=True),
-        lax.all_gather(up_cast, "fs", axis=0, tiled=True),
-    )
+    gate_full = gate_all.reshape(-1, gate_w.shape[1])
+    up_full = up_all.reshape(-1, up_w.shape[1])
     gate_sum = jnp.dot(ffn_all, gate_full, preferred_element_type=jnp.float32)
     up_sum = jnp.dot(ffn_all, up_full, preferred_element_type=jnp.float32)
     gate_pre = (gate_sum * whole_gate).astype(jnp.bfloat16)
@@ -107,7 +318,7 @@
     up_act = causal_taps(up_pre.astype(jnp.float32), up_taps) + up_bias
     hidden = (jax.nn.silu(gate_act) * up_act).astype(jnp.bfloat16)
     partial_down = column_block(
-        hidden, whole_down, lax.all_gather(down_w.astype(jnp.bfloat16), "fs", axis=1, tiled=True)
+        hidden, whole_down, down_cols
     )
     summed_two = lax.psum_scatter(
         partial_down.astype(jnp.bfloat16), "tp", scatter_dimension=0, tiled=True
@@ -142,5 +353,5 @@
         P("fs"),
     )
     return jax.shard_map(
-        local, mesh=mesh, in_specs=placed, out_specs=P(("rep", "fs"), "tp", None), check_vma=False
-    )
+        functools.partial(local, dict(mesh.shape)), mesh=mesh, in_specs=placed, out_specs=P(("rep", "fs"), "tp", None), check_vma=False
+    )

time: 589 us -> 364 us (0.62)
  waiting for transfers between devices: 390 us -> 30.8 us
  Pallas kernels: 0 us -> 215 us
  blocking collectives: 80.6 us -> 2.48 us
  matrix products: 74.4 us -> 63.6 us
  local copies, waits for them, and re-layouts: 4.21 us -> 13.6 us
    all_gather x7 -> x0, waiting for transfers between devices: 358 us -> none  [the longest x1 83.9 us: local(): lax.all_gather(up_cast, 'fs', axis=0, tiled=True)]
    pallas_call x0 -> x1, Pallas kernels: none -> 215 us  [gather_all(): pl.pallas_call(functools.partial(gather_kernel, sizes, steps, count), out...]
    unnamed x1 -> x0, blocking collectives: 40.2 us -> none
    all_gather x2 -> x0, blocking collectives: 37.9 us -> none  [the longest x1 21.6 us: local(): lax.all_gather(down_scale, 'fs', axis=0, tiled=True)]
    transpose x0 -> x2, local copies, waits for them, and re-layouts: none -> 11.2 us  [the longest x1 8.31 us: local(): down_cols = down_all.transpose(1, 0, 2).reshape(down_all.shape[1], -1)]
    all_gather x1, waiting for transfers between devices: 13.4 us -> 6.34 us  [local(): ffn_all = lax.all_gather(normed_ffn, 'tp', axis=0, tiled=True)]
  transfers between devices with their start and end apart: 11 -> 4, of which waited for: 9 -> 3; matrix products, arithmetic and copies ran while one was open for 11% -> 6% of each run, Pallas kernels for 0% -> 59%
where the time goes in v1:
time: 364 us; the launch traced here: 363 us
  Pallas kernels  215 us (59%)
  matrix products  63.6 us (17%)
  waiting for transfers between devices  30.8 us (8%)
  other arithmetic  24 us (7%)
  local copies, waits for them, and re-layouts  13.6 us (4%)
  between operations  13.4 us (4%)
    pallas_call x1, Pallas kernels, gather_all(): pl.pallas_call(functools.partial(gather_kernel, sizes, steps, count), out...  215 us
    dot_general x2, matrix products, column_block(): return jnp.dot(left, piece, preferred_element_type=jnp.float32) * scale_all  27.7 us
    reduce_scatter x1, waiting for transfers between devices, local(): lax.psum_scatter(partial_down.astype(jnp.bfloat16), 'tp', scatter_dimensi...  13.4 us
    dot_general x1, matrix products, local(): gate_sum = jnp.dot(ffn_all, gate_full, preferred_element_type=jnp.float32)  11.9 us
    reduce_scatter x1, waiting for transfers between devices, local(): lax.psum_scatter(partial_mix.astype(jnp.bfloat16), 'tp', scatter_dimensio...  11 us
    dot_general x1, matrix products, local(): up_sum = jnp.dot(ffn_all, up_full, preferred_element_type=jnp.float32)  10.3 us
    transpose x1, local copies, waits for them, and re-layouts, local(): down_cols = down_all.transpose(1, 0, 2).reshape(down_all.shape[1], -1)  8.31 us
  transfers between devices with their start and end apart: 4, of which 3 were waited for; matrix products, arithmetic and copies ran while one was open for 6% of the time, Pallas kernels for 59%

profile of v1, /device:TPU:0, one launch (start us, length us, event | category | flops | bytes accessed | tf_op | source)
XLA Modules:
  0.0 363.0 jit_solution(14902282758780130065)
XLA Ops:
  6.5 2.1 fusion.4
  8.6 0.0 copy-start.2
  8.6 3.6 fusion.6
  12.2 0.0 all-gather.3.cloned.1.call-update
  12.2 0.0 reduce-scatter.3.cloned.1.call-start
  12.3 0.0 copy-start.4
  12.3 1.2 convert_element_type.106
  13.5 0.0 copy-start.6
  13.5 1.1 convert_element_type.107
  14.7 0.0 copy-start.11
  14.7 0.0 copy-start.12
  14.7 0.0 copy-start.13
  14.7 0.0 copy-start.14
  14.7 0.0 copy-start.15
  14.7 0.0 copy-start.16
  14.7 0.0 copy-start.17
  14.7 1.8 convert_element_type.108
  16.6 1.0 convert_element_type.110.refs_3_
  17.5 0.0 copy-done.3
  17.5 0.9 convert_element_type.111.refs_4_
  18.5 1.0 convert_element_type.112.refs_5_
  19.4 0.7 convert_element_type.109.refs_2_
  20.2 0.0 copy-done.11
  20.2 0.0 copy-done.13
  20.2 0.1 concatenate.6
  20.3 0.6 pad_bitcast_fusion.refs_0_
  20.9 1.0 pad_maximum_fusion.refs_1_
  21.9 215.0 %shard_map.217 = (f32[8,24,128]{2,1,0:T(8,128)}, bf16[8,256,1536]{2,1,0:T(8,128)(2,1)}, bf16[8,512,256]{2,1,0:T(8,128)(2,1)}, bf16[8,256,1408]{2,1,0:T(8,128)(2,...) custom-call(f32[24,128]{1,0:T(8,128)} %pad_bitcast_fusion.refs_0_, ...), custom_call_target="tpu_custom_call" | custom-call | tf_op jit(solution)/shard_map/pallas_call | solution.py:192
  236.9 0.9 copy.36
  237.8 0.1 fusion.42
  237.9 0.1 mul.243
  237.9 0.1 mul.240
  238.0 0.1 mul.235
  238.1 0.1 slice_bitcast_fusion.1
  238.2 2.9 copy.28
  241.1 0.0 all-gather.3.cloned.1.call-done
  241.1 5.4 %multiply_convert_fusion.6 = bf16[1024,512]{0,1:T(8,128)(2,1)S(1)} fusion(bf16[1024,2048]{1,0:T(8,128)(2,1)} %all-gather.3.cloned.1.call-done, bf16[2048,1536]{1,0:T(8,128)(2,1)} %bitcast.57, f32[512]{0:T(512)S(1)} %mul.243), kind=kOutput, calls=%fused_computation.42 | convolution fusion | flops 2148532224 | bytes 7342080 | tf_op jit(solution)/shard_map/dot_general | solution.py:291
  246.5 4.0 %convert_multiply_fusion.6 = f32[1024,512]{0,1:T(8,128)S(1)} fusion(bf16[1024,512]{0,1:T(8,128)(2,1)S(1)} %multiply_convert_fusion.6, bf16[1024,2048]{1,0:T(8,128)(2,1)S(1)} %copy-done.18, bf16[2048,1536]{1,0:T(8,128)(2,1)} %bitcast.58, f32[512]{0:T(512)S(1)} %mul.240), kind=kOutput, calls=%fused_computation.41 | convolution fusion | flops 2150105088 | bytes 9439232 | tf_op jit(solution)/shard_map/dot_general | solution.py:288
  250.5 0.0 copy-start.22
  250.5 4.3 %fusion.16 = (f32[1024]{0:T(1024)S(1)}, bf16[1024,512]{0,1:T(8,128)(2,1)S(1)}) fusion(f32[1024,512]{0,1:T(8,128)S(1)} %convert_multiply_fusion.6, f32[512]{0:T(512)S(1)} %bitcast.55, f32[512]{0:T(512)S(1)} %bitcast.56, f32[512]{0:T(512)S(1)} %bitcast.54, f32[512]{0:T(512)S(1)} %mul.235, bf16[1024,2048]{1,0:T(8,128)(2,1)S(1)} %copy-done.18, ...), kind=kOutput, calls=%fused_computation.31 | convolution fusion | flops 2154298368 | bytes 9449472 | tf_op jit(solution)/shard_map/dot_general | solution.py:285
  254.8 2.5 psum.7
  257.3 0.0 copy-done.22
  257.3 4.5 %multiply_convert_fusion.1 = bf16[1024,2048]{1,0:T(8,128)(2,1)} fusion(bf16[512,2048]{0,1:T(8,128)(2,1)S(1)} %bitcast.46, f32[2048]{0:T(1024)S(1)} %bitcast.52, bf16[1024,512]{0,1:T(8,128)(2,1)S(1)} %get-tuple-element.34, f32[512]{0:T(512)S(1)} %copy-done.22, f32[1024]{0:T(1024)S(1)} %add_rsqrt_fusion), kind=kOutput, calls=%fused_computation.1 | convolution fusion | flops 2153775104 | bytes 7354368 | tf_op jit(solution)/shard_map/dot_general | solution.py:225
  261.8 0.0 reduce-scatter.3.cloned.1.call-update
  261.8 0.0 all-gather.5.cloned.1.call-start
  261.9 11.0 %reduce-scatter.3.cloned.1.call-done = bf16[512,2048]{1,0:T(8,128)(2,1)} async-done(((bf16[1024,2048]{1,0:T(8,128)(2,1)}), bf16[512,2048]{1,0:T(8,128)(2,1)}) %reduce-scatter.3.cloned.1.call-update) | async-done | bytes 2097168 | tf_op jit(solution)/shard_map/reduce_scatter | solution.py:304
  272.9 2.5 fusion
  275.5 2.4 fusion.2
  277.8 0.0 all-gather.5.cloned.1.call-update
  277.8 0.0 reduce-scatter.5.cloned.1.call-start
  277.9 0.1 fusion.41
  278.0 0.1 mul.270
  278.1 0.1 mul.283
  278.2 0.0 copy-start.7
  278.2 0.0 copy-start.8
  278.2 8.3 %copy.29 = bf16[1408,8,256]{0,2,1:T(8,128)(2,1)} copy(bf16[1408,8,256]{2,0,1:T(8,128)(2,1)} %bitcast.44) | data formatting | bytes 11534336 | tf_op jit(solution)/shard_map/transpose | solution.py:283
  286.5 0.1 slice_reduce_fusion.2
  286.6 6.3 %all-gather.5.cloned.1.call-done = bf16[1024,2048]{1,0:T(8,128)(2,1)} async-done(((bf16[512,2048]{1,0:T(8,128)(2,1)}), bf16[1024,2048]{1,0:T(8,128)(2,1)}) %all-gather.5.cloned.1.call-update) | async-done | bytes 4194320 | tf_op jit(solution)/shard_map/all_gather | solution.py:310
  292.9 11.9 %fusion.8 = f32[1024,1408]{1,0:T(8,128)} fusion(bf16[1024,2048]{1,0:T(8,128)(2,1)} %all-gather.5.cloned.1.call-done, bf16[2048,1408]{1,0:T(8,128)(2,1)} %bitcast.61, f32[1408]{0:T(1024)S(1)} %mul.270), kind=kOutput, calls=%fused_computation.19 | convolution fusion | flops 5909905408 | bytes 15734272 | tf_op jit(solution)/shard_map/dot_general | solution.py:313
  304.8 10.3 %fusion.9 = f32[1024,1408]{1,0:T(8,128)} fusion(bf16[1024,2048]{1,0:T(8,128)(2,1)S(1)} %copy-done.19, bf16[2048,1408]{1,0:T(8,128)(2,1)} %bitcast.60, f32[1408]{0:T(1024)S(1)} %mul.283), kind=kOutput, calls=%fused_computation.20 | convolution fusion | flops 5909905408 | bytes 15734272 | tf_op jit(solution)/shard_map/dot_general | solution.py:314
  315.1 23.2 %multiply_convert_fusion = bf16[1024,2048]{1,0:T(8,128)(2,1)} fusion(bf16[1408,2048]{0,1:T(8,128)(2,1)} %bitcast.45, f32[2048]{0:T(1024)S(1)} %bitcast.53, f32[1024,1408]{1,0:T(8,128)} %fusion.9, f32[1024,1408]{1,0:T(8,128)} %fusion.8, f32[1408]{0:T(1024)S(1)} %copy-done.20, f32[1408]{0:T(1024)S(1)} %get-tuple-element.21, f32[1408]{0:T(1024)S(1)} %get-tuple-element.22, ...), kind=kOutput, calls=%fused_computation | convolution fusion | flops 5935726592 | bytes 21549056 | tf_op jit(solution)/shard_map/dot_general | solution.py:225
  338.3 0.0 reduce-scatter.5.cloned.1.call-update
  338.3 13.4 %reduce-scatter.5.cloned.1.call-done = bf16[512,2048]{1,0:T(8,128)(2,1)} async-done(((bf16[1024,2048]{1,0:T(8,128)(2,1)}), bf16[512,2048]{1,0:T(8,128)(2,1)}) %reduce-scatter.5.cloned.1.call-update) | async-done | bytes 2097168 | tf_op jit(solution)/shard_map/reduce_scatter | solution.py:323
  351.7 4.8 %fusion.19 = bf16[1,512,2048]{2,1,0:T(8,128)(2,1)} fusion(bf16[512,2048]{1,0:T(8,128)(2,1)} %reduce-scatter.5.cloned.1.call-done, bf16[512,2048]{1,0:T(8,128)(2,1)} %reduce-scatter.3.cloned.1.call-done, bf16[1,512,2048]{2,1,0:T(8,128)(2,1)S(1)} %copy-done), kind=kLoop, calls=%fused_computation.34 | loop fusion | flops 8388608 | bytes 8388608 | tf_op jit(solution)/shard_map/broadcast_in_dim | solution.py:326
  (36 shorter events, 0.1 us)
Async XLA Ops:
  6.5 234.6 %all-gather.3.cloned.1.call-start = ((), (), s32[]{:S(2)}) async-start(), calls=%async_computation.2 | async-start | bytes 6291456 | tf_op jit(solution)/shard_map/all_gather | solution.py:256
  8.6 7.9 %copy-start.2 = (f32[256,1408]{1,0:T(8,128)S(1)}, f32[256,1408]{1,0:T(8,128)}, u32[]{:S(2)}) copy-start(f32[256,1408]{1,0:T(8,128)} %param.36) | copy-start | bytes 4325380
  12.2 5.3 %copy-start.3 = (f32[256,1408]{1,0:T(8,128)S(1)}, f32[256,1408]{1,0:T(8,128)}, u32[]{:S(2)}) copy-start(f32[256,1408]{1,0:T(8,128)} %param.37) | copy-start | bytes 4325380
  12.2 260.7 %reduce-scatter.3.cloned.1.call-start = ((), (), s32[]{:S(2)}) async-start(), calls=%async_computation.3 | async-start | bytes 6291456 | tf_op jit(solution)/shard_map/reduce_scatter | solution.py:304
  12.3 6.2 %copy-start.4 = (f32[1408,256]{1,0:T(8,128)S(1)}, f32[1408,256]{1,0:T(8,128)}, u32[]{:S(2)}) copy-start(f32[1408,256]{1,0:T(8,128)} %param.44) | copy-start | bytes 4325380
  13.5 5.9 %copy-start.6 = (f32[512,256]{1,0:T(8,128)S(1)}, f32[512,256]{1,0:T(8,128)}, u32[]{:S(2)}) copy-start(f32[512,256]{1,0:T(8,128)} %param.33) | copy-start | bytes 1572868
  14.7 5.5 %copy-start.11 = (f32[176]{0:T(256)S(1)}, f32[176]{0:T(256)}, u32[]{:S(2)}) copy-start(f32[176]{0:T(256)} %param.38) | copy-start | bytes 2116
  14.7 5.5 %copy-start.12 = (f32[176]{0:T(256)S(1)}, f32[176]{0:T(256)}, u32[]{:S(2)}) copy-start(f32[176]{0:T(256)} %param.39) | copy-start | bytes 2116
  14.7 5.5 %copy-start.13 = (f32[256]{0:T(256)S(1)}, f32[256]{0:T(256)}, u32[]{:S(2)}) copy-start(f32[256]{0:T(256)} %param.34) | copy-start | bytes 3076
  14.7 5.5 %copy-start.14 = (f32[256]{0:T(256)S(1)}, f32[256]{0:T(256)}, u32[]{:S(2)}) copy-start(f32[256]{0:T(256)} %param.45) | copy-start | bytes 3076
  14.7 5.5 %copy-start.15 = (f32[64]{0:T(128)S(1)}, f32[64]{0:T(128)}, u32[]{:S(2)}) copy-start(f32[64]{0:T(128)} %param.28) | copy-start | bytes 772
  14.7 5.5 %copy-start.16 = (f32[64]{0:T(128)S(1)}, f32[64]{0:T(128)}, u32[]{:S(2)}) copy-start(f32[64]{0:T(128)} %param.29) | copy-start | bytes 772
  14.7 5.5 %copy-start.17 = (f32[64]{0:T(128)S(1)}, f32[64]{0:T(128)}, u32[]{:S(2)}) copy-start(f32[64]{0:T(128)} %param.30) | copy-start | bytes 772
  17.5 3.4 copy-start.5
  21.9 219.2 %copy-start.10 = (f32[3,512]{1,0:T(4,128)S(1)}, f32[3,512]{1,0:T(4,128)}, u32[]{:S(2)}) copy-start(f32[3,512]{1,0:T(4,128)} %param.31) | copy-start | bytes 18436
  241.1 5.4 %copy-start.18 = (bf16[1024,2048]{1,0:T(8,128)(2,1)S(1)}, bf16[1024,2048]{1,0:T(8,128)(2,1)}, u32[]{:S(2)}) copy-start(bf16[1024,2048]{1,0:T(8,128)(2,1)} %all-gather.3.cloned.1.call-done) | copy-start | bytes 12582916
  250.5 6.8 %copy-start.22 = (f32[512]{0:T(512)S(1)}, f32[512]{0:T(512)}, u32[]{:S(2)}) copy-start(f32[512]{0:T(512)} %param.32) | copy-start | bytes 6148
  261.8 11.1 %copy-start = (bf16[1,512,2048]{2,1,0:T(8,128)(2,1)S(1)}, bf16[1,512,2048]{2,1,0:T(8,128)(2,1)}, u32[]{:S(2)}) copy-start(bf16[1,512,2048]{2,1,0:T(8,128)(2,1)} %param.23) | copy-start | bytes 6291460
  261.8 13.6 %copy-start.9 = (f32[2048]{0:T(1024)S(1)}, f32[2048]{0:T(1024)}, u32[]{:S(2)}) copy-start(f32[2048]{0:T(1024)} %param.35) | copy-start | bytes 24580
  261.8 31.1 %all-gather.5.cloned.1.call-start = ((), (), s32[]{:S(2)}) async-start(), calls=%async_computation.4 | async-start | bytes 6291456 | tf_op jit(solution)/shard_map/all_gather | solution.py:310
  272.9 2.5 copy-start.1
  277.8 73.9 %reduce-scatter.5.cloned.1.call-start = ((), (), s32[]{:S(2)}) async-start(), calls=%async_computation.5 | async-start | bytes 6291456 | tf_op jit(solution)/shard_map/reduce_scatter | solution.py:323
  278.2 8.3 %copy-start.7 = (f32[3,1408]{1,0:T(4,128)S(1)}, f32[3,1408]{1,0:T(4,128)}, u32[]{:S(2)}) copy-start(f32[3,1408]{1,0:T(4,128)} %param.41) | copy-start | bytes 50692
  278.2 8.3 %copy-start.8 = (f32[3,1408]{1,0:T(4,128)S(1)}, f32[3,1408]{1,0:T(4,128)}, u32[]{:S(2)}) copy-start(f32[3,1408]{1,0:T(4,128)} %param.40) | copy-start | bytes 50692
  292.9 11.9 %copy-start.19 = (bf16[1024,2048]{1,0:T(8,128)(2,1)S(1)}, bf16[1024,2048]{1,0:T(8,128)(2,1)}, u32[]{:S(2)}) copy-start(bf16[1024,2048]{1,0:T(8,128)(2,1)} %all-gather.5.cloned.1.call-done) | copy-start | bytes 12582916
  304.8 10.3 %copy-start.20 = (f32[1408]{0:T(1024)S(1)}, f32[1408]{0:T(1024)}, u32[]{:S(2)}) copy-start(f32[1408]{0:T(1024)} %param.43) | copy-start | bytes 16900
  304.8 10.3 %copy-start.21 = (f32[1408]{0:T(1024)S(1)}, f32[1408]{0:T(1024)}, u32[]{:S(2)}) copy-start(f32[1408]{0:T(1024)} %param.42) | copy-start | bytes 16900
Sparse Core Ops, SparseCore 0:
  12.3 16.3 all-gather.2
  262.0 10.9 reduce-scatter.2
  278.0 14.9 all-gather.4
  338.5 13.2 reduce-scatter.4
